TPU v7x, 32 devices: a whole 2x2x4 slice. The times are simulated.
32 devices in a mesh: sp: 8 (over z, x), tp: 4 (over y, core).
Axes of the slice: x: 2, y: 2, z: 4, core: 2. Of those that a mesh axis runs over, the one named last changes fastest.
Arguments:
- tokens: bfloat16 [4096, 4096], P('sp', 'tp'), may hold values from -8 to 8
- w_key: bfloat16 [4096, 2048], P(None, 'tp'), may hold values from -0.09375 to 0.09375
- w_value: bfloat16 [4096, 2048], P(None, 'tp'), may hold values from -0.09375 to 0.09375
- w_beta: bfloat16 [4096, 16], replicated, may hold values from -0.09375 to 0.09375
- w_decay: bfloat16 [4096, 16], replicated, may hold values from -0.09375 to 0.09375
- beta_bias: float32 [16], replicated, may hold values from -6 to -4
- decay_rate: float32 [16], replicated, as said below
- forgetting_increment: float32 [16, 4096], P('tp', 'sp')
- new_query: bfloat16 [16, 128], P('tp', 'sp'), may hold values from -6 to 6
- read_gain: bfloat16 [128], replicated, may hold values from 0.099609375 to 1.8984375
Outputs:
- state_cache: bfloat16 [16, 128, 128], P('tp', 'sp')
- first_read: float32 [16, 128], P('tp')
Inputs may be any that keep to these rules, and one draw needn't show every extreme that they name: `decay_rate`: positive.
All inputs are finite; a program needn't handle non-finite values.
Results may differ from a plain program's by a relative error of at most 0.0075.
Values may be sent and summed in bfloat16 or wider, within the bound.
A program may use at most 64 MiB of HBM per device.

v0:
```python
import jax
import jax.numpy as jnp
from jax import lax
from jax.sharding import PartitionSpec as P

DK = 128
DV = 128
BLOCK = 64
norm_eps = 1e-06


def prefix(part, axis, combine, identity):
    count = lax.axis_size(axis)
    place = lax.axis_index(axis)
    ahead = count - 1 - place
    gathered = lax.all_gather(part, axis)
    state = jnp.zeros_like(part) + jnp.asarray(identity, part.dtype)

    def one(lap, state):
        source = count - 1 - lap
        return combine(state, lax.dynamic_index_in_dim(gathered, source, 0, False))

    return lax.fori_loop(0, ahead, one, state)


def matmul_f32(left, right):
    return jnp.dot(left, right, precision=lax.Precision.HIGHEST)


def batched_f32(left, right):
    return jnp.einsum("hij,hjk->hik", left, right, precision=lax.Precision.HIGHEST)


def unit_inverse(lower):
    current_size = lower.shape[0]
    identity = jnp.eye(current_size, dtype=jnp.float32)
    result = identity - lower
    lower_power = lower
    covered = 2
    while covered < current_size:
        lower_power = matmul_f32(lower_power, lower_power)
        result = matmul_f32(result, identity + lower_power)
        covered = covered * 2
    return result


def block_terms(key_blk, value_blk, beta_blk, logd_blk):
    current_size = key_blk.shape[0]
    cumulative = jnp.cumsum(logd_blk)
    spread = cumulative[:, None] - cumulative[None, :]
    location_positions = jnp.arange(current_size)
    causal = location_positions[:, None] >= location_positions[None, :]
    strict = location_positions[:, None] > location_positions[None, :]
    decay_table = jnp.where(causal, jnp.exp(jnp.where(causal, spread, 0.0)), 0.0)
    key_beta = key_blk * beta_blk[:, None]
    lower = jnp.where(strict, matmul_f32(key_beta, key_blk.T) * decay_table, 0.0)
    inverse = unit_inverse(lower)
    update = matmul_f32(inverse, value_blk * beta_blk[:, None])
    erase = matmul_f32(inverse, key_beta * jnp.exp(cumulative)[:, None])
    key_remainder = key_blk * jnp.exp(cumulative[-1] - cumulative)[:, None]
    return (update, erase, key_remainder, jnp.exp(cumulative[-1]))


def per_device(
    tokens,
    w_key,
    w_value,
    w_beta,
    w_decay,
    beta_bias,
    decay_rate,
    forgetting_increment,
    new_query,
    read_gain,
):
    heads_here = w_key.shape[1] // DK
    token_count = tokens.shape[0]
    head_start = lax.axis_index("tp") * heads_here
    gate_weights = jnp.concatenate(
        [
            lax.dynamic_slice_in_dim(w_beta, head_start, heads_here, 1),
            lax.dynamic_slice_in_dim(w_decay, head_start, heads_here, 1),
        ],
        axis=1,
    )
    piece = lax.all_gather(tokens, "tp", axis=1, tiled=True)
    key_acc = jnp.dot(piece, w_key, preferred_element_type=jnp.float32)
    value_acc = jnp.dot(piece, w_value, preferred_element_type=jnp.float32)
    gate_acc = jnp.dot(piece, gate_weights, preferred_element_type=jnp.float32)
    key_wide = (
        lax.optimization_barrier(key_acc.astype(jnp.bfloat16))
        .astype(jnp.float32)
        .reshape(token_count, heads_here, DK)
    )
    key_unit = key_wide * lax.rsqrt(jnp.sum(key_wide * key_wide, axis=-1, keepdims=True) + norm_eps)
    value_wide = (
        lax.optimization_barrier(value_acc.astype(jnp.bfloat16))
        .astype(jnp.float32)
        .reshape(token_count, heads_here, DV)
    )
    bias_here = lax.dynamic_slice_in_dim(beta_bias, head_start, heads_here, 0)
    rate_here = lax.dynamic_slice_in_dim(decay_rate, head_start, heads_here, 0)
    beta = jax.nn.sigmoid(gate_acc[:, :heads_here] + bias_here).T
    log_decay = (
        -rate_here[:, None] * jax.nn.softplus(gate_acc[:, heads_here:].T) + forgetting_increment
    )
    blocks = token_count // BLOCK
    key_heads = key_unit.transpose(1, 0, 2).reshape(heads_here, blocks, BLOCK, DK)
    value_heads = value_wide.transpose(1, 0, 2).reshape(heads_here, blocks, BLOCK, DV)
    terms = jax.vmap(jax.vmap(block_terms))(
        key_heads,
        value_heads,
        beta.reshape(heads_here, blocks, BLOCK),
        log_decay.reshape(heads_here, blocks, BLOCK),
    )
    inputs = tuple((jnp.moveaxis(item, 1, 0) for item in terms))
    identity = jnp.broadcast_to(jnp.eye(DK, dtype=jnp.float32), (heads_here, DK, DK))
    value_zeros = jnp.zeros((heads_here, DK, DV), jnp.float32)
    padding = jnp.zeros((heads_here, BLOCK, DK), jnp.float32)

    def advance(state, block_in):
        update, erase, key_remainder, keep = block_in
        fresh = jnp.concatenate([update, padding], axis=-1) - jnp.einsum(
            "hcd,hde->hce", erase, state, precision=lax.Precision.HIGHEST
        )
        state = keep[:, None, None] * state + jnp.einsum(
            "hcd,hce->hde", key_remainder, fresh, precision=lax.Precision.HIGHEST
        )
        return (state, None)

    combined, _ = lax.scan(advance, jnp.concatenate([value_zeros, identity], axis=-1), inputs)
    local_b = combined[:, :, :DV]
    local_left = combined[:, :, DV:]
    later_product = prefix(local_left, "sp", batched_f32, identity)
    summed = lax.psum_scatter(
        batched_f32(later_product, local_b), "sp", scatter_dimension=1, tiled=True
    )
    own_rows = summed.astype(jnp.bfloat16)
    partial_read = jnp.sum(
        new_query.astype(jnp.float32)[:, :, None] * own_rows.astype(jnp.float32), axis=1
    )
    raw_read = lax.psum(partial_read, "sp")
    first_read = (
        raw_read
        * lax.rsqrt(jnp.mean(raw_read * raw_read, axis=-1, keepdims=True) + norm_eps)
        * read_gain.astype(jnp.float32)
    )
    return (own_rows, first_read)


def solution(mesh):
    return jax.shard_map(
        per_device,
        mesh=mesh,
        in_specs=(
            P("sp", "tp"),
            P(None, "tp"),
            P(None, "tp"),
            P(),
            P(),
            P(),
            P(),
            P("tp", "sp"),
            P("tp", "sp"),
            P(),
        ),
        out_specs=(P("tp", "sp", None), P("tp", None)),
        check_vma=False,
    )
```

profile of v0, /device:TPU:0, one launch (start us, length us, event | category | flops | bytes accessed | tf_op | source)
XLA Modules:
  0.0 263.8 jit_solution(13869263426340788410)
XLA Ops:
  11.1 35.6 %all-gather.4.cloned.1.call-done = bf16[512,4096]{1,0:T(8,128)(2,1)} async-done(((bf16[512,1024]{1,0:T(8,128)(2,1)}), bf16[512,4096]{1,0:T(8,128)(2,1)}) %all-gather.4.cloned.1.call-update) | async-done | bytes 4194320 | tf_op jit(solution)/shard_map/all_gather | solution.py:86
  46.8 3.4 %convolution_bitcast_fusion.3 = f32[512,8]{0,1:T(8,128)S(1)} fusion(bf16[512,4096]{1,0:T(8,128)(2,1)} %all-gather.4.cloned.1.call-done, bf16[4096,4]{0,1:T(4,128)(2,1)S(1)} %get-tuple-element.148, bf16[4096,4]{0,1:T(4,128)(2,1)S(1)} %get-tuple-element.149), kind=kOutput, calls=%fused_computation.25 | convolution fusion | flops 33685504 | bytes 4276224 | tf_op jit(solution)/shard_map/dot_general | solution.py:89
  52.9 5.9 %convolution_convert_fusion.1 = bf16[512,512]{1,0:T(8,128)(2,1)S(1)} fusion(bf16[512,4096]{1,0:T(8,128)(2,1)} %all-gather.4.cloned.1.call-done, bf16[4096,512]{1,0:T(8,128)(2,1)} %param.15), kind=kOutput, calls=%fused_computation.24 | convolution fusion | flops 2147745792 | bytes 8912896 | tf_op jit(solution)/shard_map/dot_general | solution.py:87
  58.8 2.3 convolution_convert_fusion
  62.7 2.1 multiply_bitcast_fusion
  64.7 2.7 %fusion.15 = f32[4,8,64,64]{3,2,1,0:T(8,128)S(1)} fusion(f32[4,8,64,128]{3,2,1,0:T(8,128)S(1)} %bitcast.101, f32[4,8,64]{2,1,0:T(8,128)S(1)} %reduce_window_sum.11, f32[4,8,64]{2,1,0:T(8,128)S(1)} %mul.102, pred[64,64]{1,0:T(8,128)(4,1)} %get-tuple-element.150, pred[64,64]{1,0:T(8,128)(4,1)} %get-tuple-element.151), kind=kOutput, calls=%fused_computation.22 | convolution fusion | flops 202244096 | bytes 1597440 | tf_op jit(solution)/shard_map/vmap(vmap())/dot_general | solution.py:27
  79.6 2.6 convolution_bitcast_fusion.1
  83.5 29.7 %while.22 = (s32[]{:T(128)}, f32[4,128,256]{2,1,0:T(8,128)S(1)}, f32[8,4]{1,0:T(8,128)}, f32[8,4,64,128]{3,2,0,1:T(8,128)}, f32[8,4,64,128]{3,2,0,1:T(8,128)S(1)}, /*index=5*/f32[8,4,64,128]{3,2,0,1:T(8,128)}, s32[]{:T(128)}) while((s32[]{:T(128)}, f32[4,128,256]{2,1,0:T(8,128)S(1)}, f32[8,4]{1,0:T(8,128)}, f32[8,4,64,128]{3,2,0,1:T(8,128)}, ...), condition=%wide.region_3.4_spmd, body=%wide.region_2.3_spmd.sunk | while | flops 201654272 | bytes 2752661 | solution.py:131
  85.5 1.7 convolution_add_fusion.3
  89.2 1.7 convolution_add_fusion.3
  92.9 1.7 convolution_add_fusion.3
  96.7 1.7 convolution_add_fusion.3
  100.4 1.7 convolution_add_fusion.3
  104.1 1.7 convolution_add_fusion.3
  107.8 1.7 convolution_add_fusion.3
  111.5 1.7 convolution_add_fusion.3
  114.0 49.2 %all-gather.6.cloned.1.call-done = f32[32,128,128]{2,1,0:T(8,128)} async-done(((f32[4,128,128]{2,1,0:T(8,128)}), f32[32,128,128]{2,1,0:T(8,128)}) %all-gather.6.cloned.1.call-update) | async-done | bytes 2097168 | tf_op jit(solution)/shard_map/all_gather | solution.py:16
  163.2 11.3 %while.23 = (s32[]{:T(128)}, f32[4,128,128]{1,2,0:T(8,128)S(1)}, s32[]{:T(128)}, f32[8,4,128,128]{3,2,1,0:T(8,128)}, s32[]{:T(128)}, /*index=5*/s32[]{:T(128)}, s32[]{:T(128)}, s32[]{:T(128)}) while((s32[]{:T(128)}, f32[4,128,128]{1,2,0:T(8,128)S(1)}, s32[]{:T(128)}, f32[8,4,128,128]{3,2,1,0:T(8,128)}, s32[]{:T(128)}, /*index=5*/s32[]{:T(128)}, ...), condition=%wide.region_5.6_spmd, body=%wide.region_4.5_spmd.sunk | while | flops 100663304 | bytes 1310863 | solution.py:23
  163.3 1.6 convolution_bitcast_fusion.5
  164.9 1.6 convolution_bitcast_fusion.5
  166.5 1.6 convolution_bitcast_fusion.5
  169.7 1.6 convolution_bitcast_fusion.5
  175.9 59.9 %reduce-scatter.2.cloned.1.call-done = f32[4,16,128]{2,1,0:T(8,128)} async-done(((f32[4,128,128]{2,1,0:T(8,128)}), f32[4,16,128]{2,1,0:T(8,128)}) %reduce-scatter.2.cloned.1.call-update) | async-done | bytes 32784 | tf_op jit(solution)/shard_map/reduce_scatter | solution.py:135
  237.1 19.4 %psum.7 = f32[4,128]{1,0:T(4,128)S(1)} all-reduce(f32[4,128]{1,0:T(4,128)S(1)} %get-tuple-element.144), channel_id=1, replica_groups=mesh['sp'=8,'tp'=4] {'sp'}, use_global_device_ids=true, to_apply=%region_8.9 | all-reduce | flops 512 | bytes 4096 | tf_op jit(solution)/shard_map/psum | solution.py:142
  (94 shorter events, 46.8 us)
Async XLA Ops:
  7.2 43.0 %copy-start.1 = (f32[4,512]{1,0:T(4,128)S(1)}, f32[4,512]{1,0:T(4,128)}, u32[]{:S(2)}) copy-start(f32[4,512]{1,0:T(4,128)} %param.21) | copy-start | bytes 24580
  7.2 39.6 %all-gather.4.cloned.1.call-start = ((), (), s32[]{:S(2)}) async-start(), calls=%async_computation.1 | async-start | bytes 5242880 | tf_op jit(solution)/shard_map/all_gather | solution.py:86
  7.9 155.3 %all-gather.6.cloned.1.call-start = ((), (), s32[]{:S(2)}) async-start(), calls=%async_computation.3 | async-start | bytes 2359296 | tf_op jit(solution)/shard_map/all_gather | solution.py:16
  52.9 5.9 %copy-start = (bf16[512,4096]{1,0:T(8,128)(2,1)S(1)}, bf16[512,4096]{1,0:T(8,128)(2,1)}, u32[]{:S(2)}) copy-start(bf16[512,4096]{1,0:T(8,128)(2,1)} %all-gather.4.cloned.1.call-done) | copy-start | bytes 12582916
  52.9 5.9 %copy-start.3 = (bf16[4096,512]{1,0:T(8,128)(2,1)S(1)}, bf16[4096,512]{1,0:T(8,128)(2,1)}, u32[]{:S(2)}) copy-start(bf16[4096,512]{1,0:T(8,128)(2,1)} %param.16) | copy-start | bytes 12582916
  113.9 61.9 %copy-start.4 = (bf16[128]{0:T(256)(128)(2,1)S(1)}, bf16[128]{0:T(256)(128)(2,1)}, u32[]{:S(2)}) copy-start(bf16[128]{0:T(256)(128)(2,1)} %param.23) | copy-start | bytes 772
  113.9 61.9 %copy-start.2 = (bf16[4,16]{1,0:T(4,128)(2,1)S(1)}, bf16[4,16]{1,0:T(4,128)(2,1)}, u32[]{:S(2)}) copy-start(bf16[4,16]{1,0:T(4,128)(2,1)} %param.22) | copy-start | bytes 388
  113.9 121.8 %reduce-scatter.2.cloned.1.call-start = ((), (), s32[]{:S(2)}) async-start(), calls=%async_computation.2 | async-start | bytes 294912 | tf_op jit(solution)/shard_map/reduce_scatter | solution.py:135
Sparse Core Ops, SparseCore 0:
  9.5 37.1 all-gather.3
  114.1 49.0 all-gather.5
  175.9 59.7 reduce-scatter.1
where the time goes:
time: 265 us; the launch traced here: 264 us
  waiting for transfers between devices  145 us (55%)
  matrix products  66.4 us (25%)
  blocking collectives  19.4 us (7%)
  between operations  14 us (5%)
  local copies, waits for them, and re-layouts  9.67 us (4%)
  other arithmetic  8.34 us (3%)
    reduce_scatter x1, waiting for transfers between devices, per_device(): lax.psum_scatter(batched_f32(later_product, local_b), 'sp', scatter_dimen...  59.9 us
    all_gather x1, waiting for transfers between devices, prefix(): gathered = lax.all_gather(part, axis)  49.2 us
    all_gather x1, waiting for transfers between devices, per_device(): piece = lax.all_gather(tokens, 'tp', axis=1, tiled=True)  35.6 us
    psum x1, blocking collectives, per_device(): raw_read = lax.psum(partial_read, 'sp')  19.4 us
    dot_general x13, matrix products, matmul_f32(): return jnp.dot(left, right, precision=lax.Precision.HIGHEST)  18.7 us
    dot_general x8, matrix products, advance(): jnp.einsum('hcd,hce->hde', key_remainder, fresh, precision=lax.Precision....  13.2 us
    dot_general x8, matrix products, batched_f32(): jnp.einsum('hij,hjk->hik', left, right, precision=lax.Precision.HIGHEST)  12.2 us
    dot_general x8, matrix products, advance(): jnp.einsum('hcd,hde->hce', erase, state, precision=lax.Precision.HIGHEST)  10.7 us
  transfers between devices with their start and end apart: 3, of which 3 were waited for; matrix products, arithmetic and copies ran while one was open for 1% of the time, Pallas kernels for 0%

commit v1 on v0

--- a/solution.py
+++ b/solution.py
@@ -1,3 +1,4 @@
+import functools
 import jax
 import jax.numpy as jnp
 from jax import lax
@@ -7,6 +8,14 @@
 DV = 128
 BLOCK = 64
 norm_eps = 1e-06
+
+
+def cover_panels_here(base_x, which_axis):
+    carry_out = lax.all_gather(base_x, which_axis)
+    return jnp.sum(carry_out, 0)
+
+
+_search_node = functools.partial(cover_panels_here, which_axis="sp")
 
 
 def prefix(part, axis, combine, identity):
@@ -139,7 +148,7 @@
     partial_read = jnp.sum(
         new_query.astype(jnp.float32)[:, :, None] * own_rows.astype(jnp.float32), axis=1
     )
-    raw_read = lax.psum(partial_read, "sp")
+    raw_read = _search_node(partial_read)
     first_read = (
         raw_read
         * lax.rsqrt(jnp.mean(raw_read * raw_read, axis=-1, keepdims=True) + norm_eps)

time: 265 us -> 272 us (1.026)
  blocking collectives: 19.4 us -> 26.1 us
    all_gather x0 -> x1, blocking collectives: none -> 26.1 us  [cover_panels_here(): carry_out = lax.all_gather(base_x, which_axis)]
    psum x1 -> x0, blocking collectives: 19.4 us -> none  [per_device(): raw_read = lax.psum(partial_read, 'sp')]
where the time goes in v1:
time: 272 us; the launch traced here: 271 us
  waiting for transfers between devices  145 us (53%)
  matrix products  66.4 us (24%)
  blocking collectives  26.1 us (10%)
  between operations  14 us (5%)
  local copies, waits for them, and re-layouts  9.67 us (4%)
  other arithmetic  8.36 us (3%)
    reduce_scatter x1, waiting for transfers between devices, per_device(): lax.psum_scatter(batched_f32(later_product, local_b), 'sp', scatter_dimen...  59.9 us
    all_gather x1, waiting for transfers between devices, prefix(): gathered = lax.all_gather(part, axis)  49.2 us
    all_gather x1, waiting for transfers between devices, per_device(): piece = lax.all_gather(tokens, 'tp', axis=1, tiled=True)  35.6 us
    all_gather x1, blocking collectives, cover_panels_here(): carry_out = lax.all_gather(base_x, which_axis)  26.1 us
    dot_general x13, matrix products, matmul_f32(): return jnp.dot(left, right, precision=lax.Precision.HIGHEST)  18.7 us
    dot_general x8, matrix products, advance(): jnp.einsum('hcd,hce->hde', key_remainder, fresh, precision=lax.Precision....  13.2 us
    dot_general x8, matrix products, batched_f32(): jnp.einsum('hij,hjk->hik', left, right, precision=lax.Precision.HIGHEST)  12.2 us
    dot_general x8, matrix products, advance(): jnp.einsum('hcd,hde->hce', erase, state, precision=lax.Precision.HIGHEST)  10.7 us
  transfers between devices with their start and end apart: 3, of which 3 were waited for; matrix products, arithmetic and copies ran while one was open for 1% of the time, Pallas kernels for 0%

profile of v1, /device:TPU:0, one launch (start us, length us, event | category | flops | bytes accessed | tf_op | source)
XLA Modules:
  0.0 270.5 jit_solution(17738130138623357495)
XLA Ops:
  11.1 35.6 %all-gather.6.cloned.1.call-done = bf16[512,4096]{1,0:T(8,128)(2,1)} async-done(((bf16[512,1024]{1,0:T(8,128)(2,1)}), bf16[512,4096]{1,0:T(8,128)(2,1)}) %all-gather.6.cloned.1.call-update) | async-done | bytes 4194320 | tf_op jit(solution)/shard_map/all_gather | solution.py:95
  46.8 3.4 %convolution_bitcast_fusion.3 = f32[512,8]{0,1:T(8,128)S(1)} fusion(bf16[512,4096]{1,0:T(8,128)(2,1)} %all-gather.6.cloned.1.call-done, bf16[4096,4]{0,1:T(4,128)(2,1)S(1)} %get-tuple-element.148, bf16[4096,4]{0,1:T(4,128)(2,1)S(1)} %get-tuple-element.149), kind=kOutput, calls=%fused_computation.25 | convolution fusion | flops 33685504 | bytes 4276224 | tf_op jit(solution)/shard_map/dot_general | solution.py:98
  52.9 5.9 %convolution_convert_fusion.1 = bf16[512,512]{1,0:T(8,128)(2,1)S(1)} fusion(bf16[512,4096]{1,0:T(8,128)(2,1)} %all-gather.6.cloned.1.call-done, bf16[4096,512]{1,0:T(8,128)(2,1)} %param.15), kind=kOutput, calls=%fused_computation.24 | convolution fusion | flops 2147745792 | bytes 8912896 | tf_op jit(solution)/shard_map/dot_general | solution.py:96
  58.8 2.3 convolution_convert_fusion
  62.7 2.1 multiply_bitcast_fusion
  64.7 2.7 fusion.15
  79.6 2.6 convolution_bitcast_fusion.1
  83.5 29.7 %while.22 = (s32[]{:T(128)}, f32[4,128,256]{2,1,0:T(8,128)S(1)}, f32[8,4]{1,0:T(8,128)}, f32[8,4,64,128]{3,2,0,1:T(8,128)}, f32[8,4,64,128]{3,2,0,1:T(8,128)S(1)}, /*index=5*/f32[8,4,64,128]{3,2,0,1:T(8,128)}, s32[]{:T(128)}) while((s32[]{:T(128)}, f32[4,128,256]{2,1,0:T(8,128)S(1)}, f32[8,4]{1,0:T(8,128)}, f32[8,4,64,128]{3,2,0,1:T(8,128)}, ...), condition=%wide.region_3.4_spmd, body=%wide.region_2.3_spmd.sunk | while | flops 201654272 | bytes 2752661 | solution.py:140
  85.5 1.7 convolution_add_fusion.3
  89.2 1.7 convolution_add_fusion.3
  92.9 1.7 convolution_add_fusion.3
  96.7 1.7 convolution_add_fusion.3
  100.4 1.7 convolution_add_fusion.3
  104.1 1.7 convolution_add_fusion.3
  107.8 1.7 convolution_add_fusion.3
  111.5 1.7 convolution_add_fusion.3
  114.0 49.2 %all-gather.8.cloned.1.call-done = f32[32,128,128]{2,1,0:T(8,128)} async-done(((f32[4,128,128]{2,1,0:T(8,128)}), f32[32,128,128]{2,1,0:T(8,128)}) %all-gather.8.cloned.1.call-update) | async-done | bytes 2097168 | tf_op jit(solution)/shard_map/all_gather | solution.py:25
  163.2 11.3 %while.23 = (s32[]{:T(128)}, f32[4,128,128]{1,2,0:T(8,128)S(1)}, s32[]{:T(128)}, f32[8,4,128,128]{3,2,1,0:T(8,128)}, s32[]{:T(128)}, /*index=5*/s32[]{:T(128)}, s32[]{:T(128)}, s32[]{:T(128)}) while((s32[]{:T(128)}, f32[4,128,128]{1,2,0:T(8,128)S(1)}, s32[]{:T(128)}, f32[8,4,128,128]{3,2,1,0:T(8,128)}, s32[]{:T(128)}, /*index=5*/s32[]{:T(128)}, ...), condition=%wide.region_5.6_spmd, body=%wide.region_4.5_spmd.sunk | while | flops 100663304 | bytes 1310863 | solution.py:32
  163.3 1.6 convolution_bitcast_fusion.5
  164.9 1.6 convolution_bitcast_fusion.5
  166.5 1.6 convolution_bitcast_fusion.5
  169.7 1.6 convolution_bitcast_fusion.5
  175.9 59.9 %reduce-scatter.2.cloned.1.call-done = f32[4,16,128]{2,1,0:T(8,128)} async-done(((f32[4,128,128]{2,1,0:T(8,128)}), f32[4,16,128]{2,1,0:T(8,128)}) %reduce-scatter.2.cloned.1.call-update) | async-done | bytes 32784 | tf_op jit(solution)/shard_map/reduce_scatter | solution.py:144
  237.1 26.1 %all-gather.2 = f32[8,4,128]{2,1,0:T(4,128)S(1)} all-gather(f32[1,4,128]{2,1,0:T(4,128)S(1)} %bitcast.106), channel_id=3, replica_groups=mesh['sp'=8,'tp'=4] {'sp'}, dimensions={0}, use_global_device_ids=true | all-gather | bytes 18432 | tf_op jit(solution)/shard_map/all_gather | solution.py:14
  (95 shorter events, 46.8 us)
Async XLA Ops:
  7.2 43.0 %copy-start.1 = (f32[4,512]{1,0:T(4,128)S(1)}, f32[4,512]{1,0:T(4,128)}, u32[]{:S(2)}) copy-start(f32[4,512]{1,0:T(4,128)} %param.21) | copy-start | bytes 24580
  7.2 39.6 %all-gather.6.cloned.1.call-start = ((), (), s32[]{:S(2)}) async-start(), calls=%async_computation.1 | async-start | bytes 5242880 | tf_op jit(solution)/shard_map/all_gather | solution.py:95
  7.9 155.3 %all-gather.8.cloned.1.call-start = ((), (), s32[]{:S(2)}) async-start(), calls=%async_computation.3 | async-start | bytes 2359296 | tf_op jit(solution)/shard_map/all_gather | solution.py:25
  52.9 5.9 %copy-start = (bf16[512,4096]{1,0:T(8,128)(2,1)S(1)}, bf16[512,4096]{1,0:T(8,128)(2,1)}, u32[]{:S(2)}) copy-start(bf16[512,4096]{1,0:T(8,128)(2,1)} %all-gather.6.cloned.1.call-done) | copy-start | bytes 12582916
  52.9 5.9 %copy-start.3 = (bf16[4096,512]{1,0:T(8,128)(2,1)S(1)}, bf16[4096,512]{1,0:T(8,128)(2,1)}, u32[]{:S(2)}) copy-start(bf16[4096,512]{1,0:T(8,128)(2,1)} %param.16) | copy-start | bytes 12582916
  113.9 61.9 %copy-start.4 = (bf16[128]{0:T(256)(128)(2,1)S(1)}, bf16[128]{0:T(256)(128)(2,1)}, u32[]{:S(2)}) copy-start(bf16[128]{0:T(256)(128)(2,1)} %param.23) | copy-start | bytes 772
  113.9 61.9 %copy-start.2 = (bf16[4,16]{1,0:T(4,128)(2,1)S(1)}, bf16[4,16]{1,0:T(4,128)(2,1)}, u32[]{:S(2)}) copy-start(bf16[4,16]{1,0:T(4,128)(2,1)} %param.22) | copy-start | bytes 388
  113.9 121.8 %reduce-scatter.2.cloned.1.call-start = ((), (), s32[]{:S(2)}) async-start(), calls=%async_computation.2 | async-start | bytes 294912 | tf_op jit(solution)/shard_map/reduce_scatter | solution.py:144
Sparse Core Ops, SparseCore 0:
  9.5 37.1 all-gather.5
  114.1 49.0 all-gather.7
  175.9 59.7 reduce-scatter.1
